TPU v7x, 256 devices: a whole 4x4x8 slice. The times are simulated.
256 devices in a mesh: kv: 32 (over z, y), tp: 8 (over x, core).
Axes of the slice: x: 4, y: 4, z: 8, core: 2. Of those that a mesh axis runs over, the one named last changes fastest.
Arguments:
- tokens: bfloat16 [16, 4, 4096], P(None, None, 'kv'), may hold values from -20 to 20
- mix_gain: float32 [4096], P('kv'), may hold values from 0.1 to 1.9
- w_query: bfloat16 [4096, 2048], P('kv', 'tp'), may hold values from -0.09375 to 0.09375
- w_key: bfloat16 [4096, 2048], P('kv', 'tp'), may hold values from -0.09375 to 0.09375
- w_value: bfloat16 [4096, 2048], P('kv', 'tp'), may hold values from -0.09375 to 0.09375
- w_forget: bfloat16 [4096, 16], replicated, may hold values from -0.09375 to 0.09375
- forget_bias: float32 [16], P('tp'), may hold values from -1 to 3
- key_cache: bfloat16 [16, 16384, 2048], P(None, 'kv', 'tp'), may hold values from -6 to 6
- value_cache: bfloat16 [16, 16384, 2048], P(None, 'kv', 'tp'), may hold values from -6 to 6
- cum_gate: float32 [16, 16, 16384], P(None, 'tp', 'kv'), may hold values from -2236.08 to 0, as said below
- lengths: int32 [16], replicated, may hold values from 1 to 16384, 65524 in all
- w_out: bfloat16 [2048, 4096], P('tp', 'kv'), may hold values from -0.125 to 0.125
- mlp_gain: float32 [4096], P('kv'), may hold values from 0.1 to 1.9
- w_gate: bfloat16 [4096, 11264], P('kv', 'tp'), may hold values from -0.09375 to 0.09375
- w_up: bfloat16 [4096, 11264], P('kv', 'tp'), may hold values from -0.09375 to 0.09375
- w_down: bfloat16 [11264, 4096], P('tp', 'kv'), may hold values from -0.0546875 to 0.0546875
Outputs:
- result: bfloat16 [16, 4, 4096], P(None, None, 'kv')
Inputs may be any that keep to these rules, and one draw needn't show every extreme that they name: `cum_gate`: never rising along positions. `lengths`: one sequence fills all 16384 positions.
All inputs are finite; a program needn't handle non-finite values.
Results may differ from a plain program's by a relative error of at most 0.02.
Values may be sent and summed in bfloat16 or wider, within the bound.
A program may use at most 64 MiB of HBM per device.

v0:
```python
import jax
import jax.numpy as jnp
from jax import lax
from jax.sharding import Mesh
from jax.sharding import PartitionSpec as P

D = 4096
KV = ("kv_0", "kv_1")
EPSILON = 1e-06
NEG_FILL = -1e30


def in_one(arrays, axis):
    flat, at, outs = (jnp.concatenate([a.reshape(-1) for a in arrays]), 0, [])
    running = lax.psum(flat, axis)
    for a in arrays:
        outs.append(running[at : at + a.size].reshape(a.shape))
        at += a.size
    return tuple(outs)


def all_in_one(array, axis):
    leaves = jax.tree.leaves(array)
    turns = sorted(range(len(leaves)), key=lambda k: -leaves[k].size)
    width = (1, *leaves[turns[0]].shape)[-1]
    lines = [
        jnp.pad(leaves[k].reshape(-1), (0, -leaves[k].size % width)).reshape(-1, width)
        for k in turns
    ]
    both, at, found = (lax.all_gather(jnp.concatenate(lines), axis), 0, {})
    for k, line in zip(turns, lines):
        share = both[:, at : at + len(line)].reshape(len(both), -1)
        found[k] = share[:, : leaves[k].size].reshape(-1, *leaves[k].shape)
        at += len(line)
    numbers = iter(range(len(leaves)))
    return jax.tree.map(lambda _: found[next(numbers)], array)


def merged_by_axis(array, axes, combine):
    for axis in axes:
        pieces = all_in_one(array, axis)
        array = jax.tree.map(lambda part: part[0], pieces)
        for k in range(1, lax.axis_size(axis)):
            array = combine(array, jax.tree.map(lambda part: part[k], pieces))
    return array


def sent_to_all(array, axis):
    peers = lax.axis_size(axis)
    return lax.all_to_all(
        jnp.broadcast_to(array[None], (peers, *array.shape)), axis, 0, 0, tiled=True
    )


def of_everyone(array, axis):
    return sent_to_all(array, axis).astype(jnp.float32).sum(axis=0)


def over_copies(array, axis):
    everything = sent_to_all(array, axis)
    return jnp.sum(everything, axis=0)


def cut_along(array, dim, peers):
    shape = array.shape
    tiles = array.reshape(*shape[:dim], peers, shape[dim] // peers, *shape[dim + 1 :])
    return jnp.moveaxis(tiles, dim, 0)


def sum_at_owner(array, axis, dim):
    tiles = cut_along(array, dim, lax.axis_size(axis))
    arrived = lax.all_to_all(tiles, axis, split_axis=0, concat_axis=0, tiled=True)
    return arrived.astype(jnp.float32).sum(axis=0)


def sent_together(arrays, axis, dim, along):
    ends, at = ([], 0)
    for a in arrays[:-1]:
        at += a.shape[along]
        ends.append(at)
    both = jnp.concatenate(arrays, axis=along)
    return tuple(jnp.split(sum_at_owner(both, axis, dim), ends, axis=along))


def joined_along(tiles, dim):
    tiles = jnp.moveaxis(tiles, 0, dim)
    shape = tiles.shape
    return tiles.reshape(*shape[:dim], shape[dim] * shape[dim + 1], *shape[dim + 2 :])


def collect(array, axis, dim):
    tiles = sent_to_all(array, axis)
    return joined_along(tiles, dim)


def on_device(
    tokens,
    mix_gain,
    w_query,
    w_key,
    w_value,
    w_forget,
    forget_bias,
    key_cache,
    value_cache,
    cum_gate,
    lengths,
    w_out,
    mlp_gain,
    w_gate,
    w_up,
    w_down,
):
    seq_count, new_count, local_width = tokens.shape
    row_count = seq_count * new_count
    heads_dev = forget_bias.shape[0]
    head_width = w_query.shape[1] // heads_dev
    pos_dev = key_cache.shape[1]
    kv_index = lax.axis_index(KV)
    tp_index = lax.axis_index("tp")
    inputs = tokens.reshape(row_count, local_width).astype(jnp.float32)
    scaled = (inputs * mix_gain).astype(jnp.bfloat16)
    forget_rows = lax.dynamic_slice_in_dim(w_forget, kv_index * local_width, local_width, 0)
    forget_cols = lax.dynamic_slice_in_dim(forget_rows, tp_index * heads_dev, heads_dev, 1)
    query_part = jnp.dot(scaled, w_query, preferred_element_type=jnp.float32)
    key_part = jnp.dot(scaled, w_key, preferred_element_type=jnp.float32)
    value_part = jnp.dot(scaled, w_value, preferred_element_type=jnp.float32)
    forget_part = jnp.dot(scaled, forget_cols, preferred_element_type=jnp.float32)
    squares = jnp.sum(inputs * inputs, axis=1)
    query_sum, key_sum, value_sum, forget_sum, square_sum = tuple(
        (
            part.astype(jnp.float32)
            for part in in_one(
                (
                    query_part.astype(jnp.bfloat16),
                    key_part.astype(jnp.bfloat16),
                    value_part.astype(jnp.bfloat16),
                    forget_part.astype(jnp.bfloat16),
                    squares.astype(jnp.bfloat16),
                ),
                KV,
            )
        )
    )
    inv_norm = lax.rsqrt(square_sum / D + EPSILON)[:, None]
    head_shape = (seq_count, new_count, heads_dev, head_width)
    query = (inv_norm * query_sum).astype(jnp.bfloat16).reshape(head_shape)
    key_new = (inv_norm * key_sum).astype(jnp.bfloat16).reshape(head_shape)
    value_new = (inv_norm * value_sum).astype(jnp.bfloat16).reshape(head_shape)
    log_forget = jax.nn.log_sigmoid(inv_norm * forget_sum + forget_bias).reshape(
        seq_count, new_count, heads_dev
    )
    score_scale = head_width ** (-0.5)
    positions = kv_index * pos_dev + jnp.arange(pos_dev, dtype=jnp.int32)
    live_rows = positions[None, :] < lengths[:, None]
    live_mask = live_rows[:, None, None, :]
    cached_keys = key_cache.reshape(seq_count, pos_dev, heads_dev, head_width)
    cached_values = value_cache.reshape(seq_count, pos_dev, heads_dev, head_width)
    scores = jnp.einsum("bthd,bphd->bthp", query, cached_keys, preferred_element_type=jnp.float32)
    scores = scores * score_scale - cum_gate[:, None]
    scores = jnp.where(live_mask, scores, NEG_FILL)
    block_peak = jnp.max(scores, axis=3)
    weights = jnp.where(live_mask, jnp.exp(scores - block_peak[..., None]), 0.0)
    block_total = jnp.sum(weights, axis=3)
    block_sum = jnp.einsum(
        "bthp,bphd->bthd",
        weights.astype(jnp.bfloat16),
        cached_values,
        preferred_element_type=jnp.float32,
    )
    last_hit = positions[None, :] == (lengths - 1)[:, None]
    last_piece = jnp.sum(jnp.where(last_hit[:, None, :], cum_gate, 0.0), axis=2)

    def combine(first, second):
        peak_both = jnp.maximum(first[0], second[0])
        first_factor = jnp.exp(first[0] - peak_both)
        second_factor = jnp.exp(second[0] - peak_both)
        return (
            peak_both,
            first[1] * first_factor + second[1] * second_factor,
            first[2] * first_factor[..., None] + second[2] * second_factor[..., None],
            first[3] + second[3],
        )

    past_peak, past_total, past_sum, last_cum = merged_by_axis(
        (block_peak, block_total, block_sum, last_piece), KV, combine
    )
    key_cum = last_cum[:, None, :] + jnp.cumsum(log_forget, axis=1)
    own_scores = (
        jnp.einsum("bthd,bshd->bths", query, key_new, preferred_element_type=jnp.float32)
        * score_scale
    )
    own_scores = own_scores - jnp.transpose(key_cum, (0, 2, 1))[:, None]
    causal = (jnp.arange(new_count)[:, None] >= jnp.arange(new_count)[None, :])[None, :, None, :]
    own_scores = jnp.where(causal, own_scores, NEG_FILL)
    peak_score = jnp.maximum(past_peak, jnp.max(own_scores, axis=3))
    past_factor = jnp.exp(past_peak - peak_score)
    own_weights = jnp.where(causal, jnp.exp(own_scores - peak_score[..., None]), 0.0)
    numerator = past_sum * past_factor[..., None] + jnp.einsum(
        "bths,bshd->bthd",
        own_weights.astype(jnp.bfloat16),
        value_new,
        preferred_element_type=jnp.float32,
    )
    denominator = past_total * past_factor + jnp.sum(own_weights, axis=3)
    attended = (
        (numerator / denominator[..., None])
        .astype(jnp.bfloat16)
        .reshape(row_count, heads_dev * head_width)
    )
    attn_out = of_everyone(
        jnp.dot(attended, w_out, preferred_element_type=jnp.float32).astype(jnp.bfloat16), "tp"
    ).astype(jnp.float32)
    middle = (inputs + attn_out).astype(jnp.bfloat16)
    middle_wide = middle.astype(jnp.float32)
    squares2 = jnp.sum(middle_wide * middle_wide, axis=1)
    scaled2 = (middle_wide * mlp_gain).astype(jnp.bfloat16)
    gate_part = jnp.dot(scaled2, w_gate, preferred_element_type=jnp.float32)
    up_part = jnp.dot(scaled2, w_up, preferred_element_type=jnp.float32)
    kv_count = lax.axis_size(KV)
    share_rows = (row_count + kv_count - 1) // kv_count
    square_sum2 = over_copies(squares2, KV)
    gate_share, up_share = sent_together(
        (gate_part.astype(jnp.bfloat16), up_part.astype(jnp.bfloat16)), KV, 0, 1
    )
    share_squares = lax.dynamic_slice_in_dim(square_sum2, kv_index * share_rows, share_rows, 0)
    inv_norm2 = lax.rsqrt(share_squares / D + EPSILON)[:, None]
    hidden_share = (jax.nn.silu(inv_norm2 * gate_share) * (inv_norm2 * up_share)).astype(
        jnp.bfloat16
    )
    down_full = jnp.dot(collect(hidden_share, KV, 0), w_down, preferred_element_type=jnp.float32)
    mixed = of_everyone(down_full.astype(jnp.bfloat16), "tp").astype(jnp.float32)
    return (middle_wide + mixed).astype(jnp.bfloat16).reshape(seq_count, new_count, local_width)


def solution(mesh):
    split = Mesh(mesh.devices.reshape(8, 4, mesh.shape["tp"]), ("kv_0", "kv_1", "tp"))
    return jax.shard_map(
        on_device,
        mesh=split,
        in_specs=(
            P(None, None, KV),
            P(KV),
            P(KV, "tp"),
            P(KV, "tp"),
            P(KV, "tp"),
            P(),
            P("tp"),
            P(None, KV, "tp"),
            P(None, KV, "tp"),
            P(None, "tp", KV),
            P(),
            P("tp", KV),
            P(KV),
            P(KV, "tp"),
            P(KV, "tp"),
            P("tp", KV),
        ),
        out_specs=P(None, None, KV),
        check_vma=False,
    )
```

profile of v0, /device:TPU:1, one launch (start us, length us, event | category | flops | bytes accessed | tf_op | source)
XLA Modules:
  0.0 287.4 jit_solution(13230378988156012620)
XLA Ops:
  6.5 0.9 multiply_reduce_fusion
  7.5 0.7 multiply_convert_fusion.1
  8.3 0.9 convolution_convert_fusion.7
  9.4 1.0 fusion.23
  10.4 1.0 fusion.22
  11.5 1.0 fusion.21
  14.3 0.7 broadcast_compare_fusion.1
  15.0 1.0 select_reduce_fusion
  16.1 139.1 %all-reduce.4.cloned.1.call-done = bf16[49344]{0:T(1024)(128)(2,1)} async-done(((bf16[49344]{0:T(1024)(128)(2,1)}), bf16[49344]{0:T(1024)(128)(2,1)}) %all-reduce.4.cloned.1.call-update) | async-done | bytes 98704 | tf_op jit(solution)/shard_map/psum | solution.py:15
  155.2 0.7 fusion.103
  156.0 0.8 fusion.122
  157.0 3.5 %fusion.123 = (f32[16,4,2]{1,2,0:T(2,128)S(1)}, f32[16,4,2,512]{3,1,2,0:T(4,128)S(1)}) fusion(f32[16,2,512]{2,1,0:T(2,128)} %param.25, bf16[16,4,2,128]{3,0,2,1:T(8,128)(2,1)S(1)} %get-tuple-element.61, pred[16,512]{1,0:T(8,128)(4,1)S(1)} %get-tuple-element.62, bf16[16,512,256]{2,1,0:T(8,128)(2,1)} %param.23), kind=kOutput, calls=%fused_computation.233 | convolution fusion | flops 17039232 | bytes 4563456 | tf_op jit(solution)/shard_map/bthd,bphd->bthp/dot_general | solution.py:159
  161.0 2.9 %fusion.18 = f32[16,4,2,128]{3,1,2,0:T(4,128)S(1)} fusion(f32[16,4,2,512]{3,1,2,0:T(4,128)S(1)} %get-tuple-element.65, f32[16,4,2]{1,2,0:T(2,128)S(1)} %get-tuple-element.64, pred[16,512]{1,0:T(8,128)(4,1)S(1)} %get-tuple-element.62, bf16[16,512,256]{2,1,0:T(8,128)(2,1)} %param.24), kind=kOutput, calls=%fused_computation.12 | convolution fusion | flops 16973824 | bytes 4530688 | tf_op jit(solution)/shard_map/bthp,bphd->bthd/dot_general | solution.py:165
  164.5 19.4 %all-gather.2 = f32[8,131,128]{2,1,0:T(8,128)S(1)} all-gather(f32[1,131,128]{2,1,0:T(8,128)S(1)} %maximum_bitcast_fusion), channel_id=2, replica_groups=mesh['kv_0'=8,'kv_1'=4,'tp'=8] {'kv_0'}, dimensions={0}, use_global_device_ids=true | all-gather | bytes 603648 | tf_op jit(solution)/shard_map/all_gather | solution.py:30
  184.4 9.9 %all-gather.3 = f32[4,131,128]{2,1,0:T(8,128)S(1)} all-gather(f32[1,131,128]{2,1,0:T(8,128)S(1)} %maximum_bitcast_fusion.1), channel_id=3, replica_groups=mesh['kv_0'=8,'kv_1'=4,'tp'=8] {'kv_1'}, dimensions={0}, use_global_device_ids=true | all-gather | bytes 335360 | tf_op jit(solution)/shard_map/all_gather | solution.py:30
  194.4 0.7 slice_convert_fusion
  199.3 22.9 %all_to_all.26 = bf16[8,64,128]{2,1,0:T(8,128)(2,1)S(1)} all-to-all(bf16[8,64,128]{2,1,0:T(8,128)(2,1)S(1)} %broadcast_in_dim.71), channel_id=1, replica_groups=mesh['kv_0'=8,'kv_1'=4,'tp'=8] {'tp'}, dimensions={0} | all-to-all | bytes 262144 | tf_op jit(solution)/shard_map/all_to_all | solution.py:50
  223.0 5.5 %all-to-all-start.1 = ((f32[32,1,64]{2,1,0:T(1,128)}), f32[32,1,64]{2,1,0:T(1,128)S(1)}, u32[]{:S(2)}, u32[]{:S(2)}) async-start(f32[32,1,64]{2,1,0:T(1,128)} %broadcast_in_dim.73), calls=%async_computation.1 | async-start | bytes 32768 | tf_op jit(solution)/shard_map/all_to_all | solution.py:50
  229.0 0.9 reshape.1208
  229.8 7.2 %all-to-all-done.1 = f32[32,1,64]{2,1,0:T(1,128)S(1)} async-done(((f32[32,1,64]{2,1,0:T(1,128)}), f32[32,1,64]{2,1,0:T(1,128)S(1)}, u32[]{:S(2)}, u32[]{:S(2)}) %all-to-all-start.1) | async-done | bytes 8224 | tf_op jit(solution)/shard_map/all_to_all | solution.py:50
  237.0 3.9 %all-to-all-start.2 = ((bf16[32,2,2816]{2,1,0:T(2,128)(2,1)}), bf16[32,2,2816]{2,1,0:T(2,128)(2,1)S(1)}, u32[]{:S(2)}, u32[]{:S(2)}) async-start(bf16[32,2,2816]{2,1,0:T(2,128)(2,1)} %reshape.1208), calls=%async_computation.2 | async-start | bytes 720896 | tf_op jit(solution)/shard_map/all_to_all | solution.py:72
  241.0 11.1 %all-to-all-done.2 = bf16[32,2,2816]{2,1,0:T(2,128)(2,1)S(1)} async-done(((bf16[32,2,2816]{2,1,0:T(2,128)(2,1)}), bf16[32,2,2816]{2,1,0:T(2,128)(2,1)S(1)}, u32[]{:S(2)}, u32[]{:S(2)}) %all-to-all-start.2) | async-done | bytes 360480 | tf_op jit(solution)/shard_map/all_to_all | solution.py:72
  252.6 15.6 %all_to_all.27 = bf16[32,2,1408]{2,1,0:T(2,128)(2,1)S(1)} all-to-all(bf16[32,2,1408]{2,1,0:T(2,128)(2,1)S(1)} %broadcast_in_dim.74), channel_id=1, replica_groups=mesh['kv_0'=8,'kv_1'=4,'tp'=8] {'kv_0','kv_1'}, dimensions={0} | all-to-all | bytes 360448 | tf_op jit(solution)/shard_map/all_to_all | solution.py:50
  268.5 11.4 %all_to_all.28 = bf16[8,64,128]{2,1,0:T(8,128)(2,1)S(1)} all-to-all(bf16[8,64,128]{2,1,0:T(8,128)(2,1)S(1)} %broadcast_in_dim.75), channel_id=1, replica_groups=mesh['kv_0'=8,'kv_1'=4,'tp'=8] {'tp'}, dimensions={0} | all-to-all | bytes 262144 | tf_op jit(solution)/shard_map/all_to_all | solution.py:50
  (122 shorter events, 11.0 us)
Async XLA Ops:
  6.5 222.0 %copy-start = (bf16[128,1408]{1,0:T(8,128)(2,1)S(1)}, bf16[128,1408]{1,0:T(8,128)(2,1)}, u32[]{:S(2)}) copy-start(bf16[128,1408]{1,0:T(8,128)(2,1)} %param.30) | copy-start | bytes 1081348
  6.5 148.6 %all-reduce.4.cloned.1.call-start = ((), (), s32[]{:S(2)}) async-start(), calls=%async_computation.5 | async-start | bytes 200704 | tf_op jit(solution)/shard_map/psum | solution.py:15
  12.9 0.6 copy-start.4
  160.5 35.1 %copy-start.6 = (f32[2]{0:T(128)S(1)}, f32[2]{0:T(128)}, u32[]{:S(2)}) copy-start(f32[2]{0:T(128)} %param.22) | copy-start | bytes 28
  161.0 38.1 %copy-start.5 = (bf16[256,128]{1,0:T(8,128)(2,1)S(1)}, bf16[256,128]{1,0:T(8,128)(2,1)}, u32[]{:S(2)}) copy-start(bf16[256,128]{1,0:T(8,128)(2,1)} %param.27) | copy-start | bytes 196612
  161.0 61.2 %copy-start.3 = (bf16[16,4,128]{2,1,0:T(4,128)(2,1)S(1)}, bf16[16,4,128]{2,1,0:T(4,128)(2,1)}, u32[]{:S(2)}) copy-start(bf16[16,4,128]{2,1,0:T(4,128)(2,1)} %param.16) | copy-start | bytes 49156
  161.0 67.4 %copy-start.7 = (f32[128]{0:T(128)S(1)}, f32[128]{0:T(128)}, u32[]{:S(2)}) copy-start(f32[128]{0:T(128)} %param.28) | copy-start | bytes 1540
  164.0 64.7 %copy-start.1 = (bf16[128,1408]{1,0:T(8,128)(2,1)S(1)}, bf16[128,1408]{1,0:T(8,128)(2,1)}, u32[]{:S(2)}) copy-start(bf16[128,1408]{1,0:T(8,128)(2,1)} %param.29) | copy-start | bytes 1081348
  184.4 83.9 %copy-start.2 = (bf16[1408,128]{1,0:T(8,128)(2,1)S(1)}, bf16[1408,128]{1,0:T(8,128)(2,1)}, u32[]{:S(2)}) copy-start(bf16[1408,128]{1,0:T(8,128)(2,1)} %param.31) | copy-start | bytes 1081348
  223.0 14.0 %all-to-all-start.1 = ((f32[32,1,64]{2,1,0:T(1,128)}), f32[32,1,64]{2,1,0:T(1,128)S(1)}, u32[]{:S(2)}, u32[]{:S(2)}) async-start(f32[32,1,64]{2,1,0:T(1,128)} %broadcast_in_dim.73), calls=%async_computation.1 | async-start | bytes 32768 | tf_op jit(solution)/shard_map/all_to_all | solution.py:50
  237.0 15.1 %all-to-all-start.2 = ((bf16[32,2,2816]{2,1,0:T(2,128)(2,1)}), bf16[32,2,2816]{2,1,0:T(2,128)(2,1)S(1)}, u32[]{:S(2)}, u32[]{:S(2)}) async-start(bf16[32,2,2816]{2,1,0:T(2,128)(2,1)} %reshape.1208), calls=%async_computation.2 | async-start | bytes 720896 | tf_op jit(solution)/shard_map/all_to_all | solution.py:72
Sparse Core Ops, SparseCore 0:
  13.7 141.4 all-reduce.3
where the time goes:
time: 288 us; the launch traced here: 287 us
  waiting for transfers between devices  157 us (55%)
  blocking collectives  79.1 us (27%)
  between operations  14 us (5%)
  matrix products  11.2 us (4%)
  starting transfers between devices  9.34 us (3%)
  other arithmetic  8.2 us (3%)
  local copies, waits for them, and re-layouts  8.08 us (3%)
    psum x1, waiting for transfers between devices, in_one(): running = lax.psum(flat, axis)  139 us
    all_to_all x3, blocking collectives, sent_to_all(): lax.all_to_all(jnp.broadcast_to(array[None], (peers, *array.shape)), axis...  49.8 us
    all_gather x2, blocking collectives, all_in_one(): both, at, found = (lax.all_gather(jnp.concatenate(lines), axis), 0, {})  29.3 us
    all_to_all x1, waiting for transfers between devices, sum_at_owner(): lax.all_to_all(tiles, axis, split_axis=0, concat_axis=0, tiled=True)  11.1 us
    all_to_all x1, waiting for transfers between devices, sent_to_all(): lax.all_to_all(jnp.broadcast_to(array[None], (peers, *array.shape)), axis...  7.18 us
  transfers between devices with their start and end apart: 3, of which 3 were waited for; matrix products, arithmetic and copies ran while one was open for 1% of the time, Pallas kernels for 0%

commit v1 on v0

--- a/solution.py
+++ b/solution.py
@@ -12,7 +12,7 @@
 
 def in_one(arrays, axis):
     flat, at, outs = (jnp.concatenate([a.reshape(-1) for a in arrays]), 0, [])
-    running = lax.psum(flat, axis)
+    running = jnp.sum(lax.all_gather(flat, axis), axis=0)
     for a in arrays:
         outs.append(running[at : at + a.size].reshape(a.shape))
         at += a.size

time: 288 us -> 318 us (1.10)
  waiting for transfers between devices: 157 us -> 177 us
  local copies, waits for them, and re-layouts: 8.08 us -> 17.5 us
    unnamed x1 -> x2, waiting for transfers between devices: 0.02 us -> 158 us
    psum x1 -> x0, waiting for transfers between devices: 139 us -> none  [in_one(): running = lax.psum(flat, axis)]
    unnamed x23 -> x32, local copies, waits for them, and re-layouts: 1.05 us -> 6.39 us
    all_gather x0 -> x1, local copies, waits for them, and re-layouts: none -> 4.05 us  [in_one(): running = jnp.sum(lax.all_gather(flat, axis), axis=0)]
where the time goes in v1:
time: 318 us; the launch traced here: 317 us
  waiting for transfers between devices  177 us (56%)
  blocking collectives  78.9 us (25%)
  local copies, waits for them, and re-layouts  17.5 us (6%)
  between operations  14.7 us (5%)
  matrix products  11.2 us (4%)
  starting transfers between devices  9.22 us (3%)
  other arithmetic  8.83 us (3%)
    unnamed x2, waiting for transfers between devices  158 us
    all_to_all x3, blocking collectives, sent_to_all(): lax.all_to_all(jnp.broadcast_to(array[None], (peers, *array.shape)), axis...  49.5 us
    all_gather x2, blocking collectives, all_in_one(): both, at, found = (lax.all_gather(jnp.concatenate(lines), axis), 0, {})  29.5 us
    all_to_all x1, waiting for transfers between devices, sum_at_owner(): lax.all_to_all(tiles, axis, split_axis=0, concat_axis=0, tiled=True)  11.1 us
    all_to_all x1, waiting for transfers between devices, sent_to_all(): lax.all_to_all(jnp.broadcast_to(array[None], (peers, *array.shape)), axis...  7.64 us
    unnamed x32, local copies, waits for them, and re-layouts  6.39 us
  transfers between devices with their start and end apart: 3, of which 3 were waited for; matrix products, arithmetic and copies ran while one was open for 1% of the time, Pallas kernels for 0%

profile of v1, /device:TPU:1, one launch (start us, length us, event | category | flops | bytes accessed | tf_op | source)
XLA Modules:
  0.0 317.0 jit_solution(4360595918905964072)
XLA Ops:
  6.5 0.9 multiply_reduce_fusion
  7.4 1.3 multiply_convert_fusion.1
  8.8 1.0 fusion.21
  9.8 1.0 fusion.22
  10.8 1.0 fusion.23
  11.8 0.9 convolution_convert_fusion.7
  13.1 1.3 dynamic-slice
  16.4 2.2 dynamic-update-slice
  18.5 1.7 copy-done.1
  20.4 1.0 select_reduce_fusion
  21.4 157.9 %all-reduce.5.cloned.1.call-done = bf16[1579008]{0:T(1024)(128)(2,1)} async-done(((bf16[1579008]{0:T(1024)(128)(2,1)}), bf16[1579008]{0:T(1024)(128)(2,1)}) %all-reduce.5.cloned.1.call-update) | async-done | bytes 3158032
  179.3 4.1 %reshape.1218 = bf16[32,49344]{1,0:T(8,128)(2,1)S(1)} reshape(bf16[1579008]{0:T(1024)(128)(2,1)} %all-reduce.5.cloned.1.call-done) | data formatting | bytes 6316032 | tf_op jit(solution)/shard_map/all_gather | solution.py:15
  183.4 1.4 reduce_sum.98
  187.2 3.5 %fusion.123 = (f32[16,4,2]{1,2,0:T(2,128)S(1)}, f32[16,4,2,512]{3,1,2,0:T(4,128)S(1)}) fusion(f32[16,2,512]{2,1,0:T(2,128)} %param.25, bf16[16,4,2,128]{3,0,2,1:T(8,128)(2,1)S(1)} %get-tuple-element.61, pred[16,512]{1,0:T(8,128)(4,1)S(1)} %get-tuple-element.62, bf16[16,512,256]{2,1,0:T(8,128)(2,1)} %param.23), kind=kOutput, calls=%fused_computation.233 | convolution fusion | flops 17039232 | bytes 4563456 | tf_op jit(solution)/shard_map/bthd,bphd->bthp/dot_general | solution.py:159
  191.7 2.9 fusion.18
  194.7 19.9 %all-gather.3 = f32[8,131,128]{2,1,0:T(8,128)S(1)} all-gather(f32[1,131,128]{2,1,0:T(8,128)S(1)} %maximum_bitcast_fusion), channel_id=3, replica_groups=mesh['kv_0'=8,'kv_1'=4,'tp'=8] {'kv_0'}, dimensions={0}, use_global_device_ids=true | all-gather | bytes 603648 | tf_op jit(solution)/shard_map/all_gather | solution.py:30
  215.2 9.5 %all-gather.4 = f32[4,131,128]{2,1,0:T(8,128)S(1)} all-gather(f32[1,131,128]{2,1,0:T(8,128)S(1)} %maximum_bitcast_fusion.1), channel_id=4, replica_groups=mesh['kv_0'=8,'kv_1'=4,'tp'=8] {'kv_1'}, dimensions={0}, use_global_device_ids=true | all-gather | bytes 335360 | tf_op jit(solution)/shard_map/all_gather | solution.py:30
  228.9 22.5 %all_to_all.26 = bf16[8,64,128]{2,1,0:T(8,128)(2,1)S(1)} all-to-all(bf16[8,64,128]{2,1,0:T(8,128)(2,1)S(1)} %broadcast_in_dim.71), channel_id=1, replica_groups=mesh['kv_0'=8,'kv_1'=4,'tp'=8] {'tp'}, dimensions={0} | all-to-all | bytes 262144 | tf_op jit(solution)/shard_map/all_to_all | solution.py:50
  252.8 5.3 %all-to-all-start.1 = ((f32[32,1,64]{2,1,0:T(1,128)}), f32[32,1,64]{2,1,0:T(1,128)S(1)}, u32[]{:S(2)}, u32[]{:S(2)}) async-start(f32[32,1,64]{2,1,0:T(1,128)} %broadcast_in_dim.73), calls=%async_computation.1 | async-start | bytes 32768 | tf_op jit(solution)/shard_map/all_to_all | solution.py:50
  259.0 7.6 %all-to-all-done.1 = f32[32,1,64]{2,1,0:T(1,128)S(1)} async-done(((f32[32,1,64]{2,1,0:T(1,128)}), f32[32,1,64]{2,1,0:T(1,128)S(1)}, u32[]{:S(2)}, u32[]{:S(2)}) %all-to-all-start.1) | async-done | bytes 8224 | tf_op jit(solution)/shard_map/all_to_all | solution.py:50
  266.6 3.9 %all-to-all-start.2 = ((bf16[32,2,2816]{2,1,0:T(2,128)(2,1)}), bf16[32,2,2816]{2,1,0:T(2,128)(2,1)S(1)}, u32[]{:S(2)}, u32[]{:S(2)}) async-start(bf16[32,2,2816]{2,1,0:T(2,128)(2,1)} %reshape.1208), calls=%async_computation.2 | async-start | bytes 720896 | tf_op jit(solution)/shard_map/all_to_all | solution.py:72
  270.6 11.1 %all-to-all-done.2 = bf16[32,2,2816]{2,1,0:T(2,128)(2,1)S(1)} async-done(((bf16[32,2,2816]{2,1,0:T(2,128)(2,1)}), bf16[32,2,2816]{2,1,0:T(2,128)(2,1)S(1)}, u32[]{:S(2)}, u32[]{:S(2)}) %all-to-all-start.2) | async-done | bytes 360480 | tf_op jit(solution)/shard_map/all_to_all | solution.py:72
  282.3 15.6 %all_to_all.27 = bf16[32,2,1408]{2,1,0:T(2,128)(2,1)S(1)} all-to-all(bf16[32,2,1408]{2,1,0:T(2,128)(2,1)S(1)} %broadcast_in_dim.74), channel_id=1, replica_groups=mesh['kv_0'=8,'kv_1'=4,'tp'=8] {'kv_0','kv_1'}, dimensions={0} | all-to-all | bytes 360448 | tf_op jit(solution)/shard_map/all_to_all | solution.py:50
  298.1 11.4 %all_to_all.28 = bf16[8,64,128]{2,1,0:T(8,128)(2,1)S(1)} all-to-all(bf16[8,64,128]{2,1,0:T(8,128)(2,1)S(1)} %broadcast_in_dim.75), channel_id=1, replica_groups=mesh['kv_0'=8,'kv_1'=4,'tp'=8] {'tp'}, dimensions={0} | all-to-all | bytes 262144 | tf_op jit(solution)/shard_map/all_to_all | solution.py:50
  (133 shorter events, 13.6 us)
Async XLA Ops:
  6.5 245.0 %copy-start = (bf16[128,1408]{1,0:T(8,128)(2,1)S(1)}, bf16[128,1408]{1,0:T(8,128)(2,1)}, u32[]{:S(2)}) copy-start(bf16[128,1408]{1,0:T(8,128)(2,1)} %param.30) | copy-start | bytes 1081348
  6.5 13.7 %copy-start.10 = (s32[16]{0:T(128)S(1)}, s32[16]{0:T(128)}, u32[]{:S(2)}) copy-start(s32[16]{0:T(128)} %param.26) | copy-start | bytes 196
  6.5 172.8 %all-reduce.5.cloned.1.call-start = ((), (), s32[]{:S(2)}) async-start(), calls=%async_computation.5 | async-start | bytes 6316032
  15.5 0.6 copy-start.5
  18.5 1.7 copy-start.1
  190.7 34.3 %copy-start.8 = (f32[2]{0:T(128)S(1)}, f32[2]{0:T(128)}, u32[]{:S(2)}) copy-start(f32[2]{0:T(128)} %param.22) | copy-start | bytes 28
  191.7 37.1 %copy-start.7 = (bf16[256,128]{1,0:T(8,128)(2,1)S(1)}, bf16[256,128]{1,0:T(8,128)(2,1)}, u32[]{:S(2)}) copy-start(bf16[256,128]{1,0:T(8,128)(2,1)} %param.27) | copy-start | bytes 196612
  191.7 59.8 %copy-start.6 = (f32[64,128]{1,0:T(8,128)S(1)}, f32[64,128]{1,0:T(8,128)}, u32[]{:S(2)}) copy-start(f32[64,128]{1,0:T(8,128)} %get-tuple-element.34) | copy-start | bytes 98308
  191.7 59.8 %copy-start.9 = (f32[128]{0:T(128)S(1)}, f32[128]{0:T(128)}, u32[]{:S(2)}) copy-start(f32[128]{0:T(128)} %param.28) | copy-start | bytes 1540
  194.7 57.1 %copy-start.2 = (bf16[128,1408]{1,0:T(8,128)(2,1)S(1)}, bf16[128,1408]{1,0:T(8,128)(2,1)}, u32[]{:S(2)}) copy-start(bf16[128,1408]{1,0:T(8,128)(2,1)} %param.29) | copy-start | bytes 1081348
  194.7 57.3 %copy-start.4 = (bf16[16,4,128]{2,1,0:T(4,128)(2,1)S(1)}, bf16[16,4,128]{2,1,0:T(4,128)(2,1)}, u32[]{:S(2)}) copy-start(bf16[16,4,128]{2,1,0:T(4,128)(2,1)} %param.16) | copy-start | bytes 49156
  215.1 82.8 %copy-start.3 = (bf16[1408,128]{1,0:T(8,128)(2,1)S(1)}, bf16[1408,128]{1,0:T(8,128)(2,1)}, u32[]{:S(2)}) copy-start(bf16[1408,128]{1,0:T(8,128)(2,1)} %param.31) | copy-start | bytes 1081348
  252.8 13.9 %all-to-all-start.1 = ((f32[32,1,64]{2,1,0:T(1,128)}), f32[32,1,64]{2,1,0:T(1,128)S(1)}, u32[]{:S(2)}, u32[]{:S(2)}) async-start(f32[32,1,64]{2,1,0:T(1,128)} %broadcast_in_dim.73), calls=%async_computation.1 | async-start | bytes 32768 | tf_op jit(solution)/shard_map/all_to_all | solution.py:50
  266.6 15.1 %all-to-all-start.2 = ((bf16[32,2,2816]{2,1,0:T(2,128)(2,1)}), bf16[32,2,2816]{2,1,0:T(2,128)(2,1)S(1)}, u32[]{:S(2)}, u32[]{:S(2)}) async-start(bf16[32,2,2816]{2,1,0:T(2,128)(2,1)} %reshape.1208), calls=%async_computation.2 | async-start | bytes 720896 | tf_op jit(solution)/shard_map/all_to_all | solution.py:72
Sparse Core Ops, SparseCore 0:
  20.4 158.8 all-reduce.4
